TPU v7x, 32 devices: a whole 2x2x4 slice. The times are simulated.
32 devices in a mesh: sp: 8 (over z, y), tp: 4 (over x, core).
Axes of the slice: x: 2, y: 2, z: 4, core: 2. Of those that a mesh axis runs over, the one named last changes fastest.
Arguments:
- tokens: bfloat16 [4096, 2048], P(('sp', 'tp')), may hold values from -6 to 6
- queries: bfloat16 [4096, 1024], P('sp', 'tp'), may hold values from -160 to 160
- keys: bfloat16 [4096, 1024], P('sp', 'tp'), may hold values from -8 to 8
- values: bfloat16 [4096, 1024], P('sp', 'tp'), may hold values from -6 to 6
- lambdas: float32 [8], P('tp'), may hold values from 0.3 to 0.8
- head_gain: float32 [128], replicated, may hold values from 0.1 to 1.9
- out_weight: bfloat16 [1024, 2048], replicated, may hold values from -0.1875 to 0.1875
- mixer_gain: float32 [2048], replicated, may hold values from 0.1 to 1.9
- up_weight: bfloat16 [2048, 4096], P('sp', 'tp'), may hold values from -0.125 to 0.125
- down_weight: bfloat16 [4096, 2048], P('tp', 'sp'), may hold values from -0.09375 to 0.09375
Outputs:
- result: bfloat16 [4096, 2048], P(('sp', 'tp'))
All inputs are finite; a program needn't handle non-finite values.
Results may differ from a plain program's by a relative error of at most 0.02.
Values may be sent and summed in bfloat16 or wider, within the bound.
A program may use at most 128 MiB of HBM per device.

v0:
```python
import math
import jax
import jax.numpy as jnp
from jax import lax
from jax.sharding import PartitionSpec as P

DQK = 64
DV = 128


def per_device(
    tokens,
    queries,
    keys,
    values,
    lambdas,
    head_gain,
    out_weight,
    mixer_gain,
    up_weight,
    down_weight,
):
    tok_rows = queries.shape[0]
    head_count = lambdas.shape[0]
    scaling = DQK ** (-0.5)
    sp_index = lax.axis_index("sp")
    first_row = sp_index * tok_rows
    last_row = first_row + tok_rows - 1
    query_split = queries.reshape(tok_rows, head_count, 2, DQK)
    query_pos = first_row + lax.broadcasted_iota(jnp.int32, (tok_rows, 1), 0)
    floor_max = jnp.full((head_count, tok_rows), -1e30, jnp.float32)
    zero_total = jnp.zeros((head_count, tok_rows), jnp.float32)
    zero_acc = jnp.zeros((head_count, tok_rows, DV), jnp.float32)
    start_state = (floor_max, zero_total, zero_acc, floor_max, zero_total, zero_acc)
    key_piece = lax.all_gather(keys, "sp", axis=0, tiled=True)
    value_piece = lax.all_gather(values, "sp", axis=0, tiled=True)
    piece_rows = key_piece.shape[0]
    block_width = math.gcd(piece_rows, 512)

    def one_block(block_index, running):
        offset = block_index * block_width

        def update(inner):
            key_block = lax.dynamic_slice_in_dim(key_piece, offset, block_width, 0).reshape(
                block_width, head_count, 2, DQK
            )
            value_block = lax.dynamic_slice_in_dim(value_piece, offset, block_width, 0).reshape(
                block_width, head_count, DV
            )
            key_pos = offset + lax.broadcasted_iota(jnp.int32, (1, block_width), 1)
            allowed = key_pos <= query_pos
            updated = []
            for map_index in range(2):
                run_max = inner[3 * map_index]
                run_total = inner[3 * map_index + 1]
                run_acc = inner[3 * map_index + 2]
                scores = (
                    jnp.einsum(
                        "qhd,khd->hqk",
                        query_split[:, :, map_index],
                        key_block[:, :, map_index],
                        preferred_element_type=jnp.float32,
                    )
                    * scaling
                )
                scores = jnp.where(allowed[None], scores, -jnp.inf)
                new_max = jnp.maximum(run_max, jnp.max(scores, axis=2))
                shrink = jnp.exp(run_max - new_max)
                exponent = jnp.exp(scores - new_max[:, :, None])
                new_total = run_total * shrink + jnp.sum(exponent, axis=2)
                new_acc = run_acc * shrink[:, :, None] + jnp.einsum(
                    "hqk,khd->hqd",
                    exponent.astype(jnp.bfloat16),
                    value_block,
                    preferred_element_type=jnp.float32,
                )
                updated += [new_max, new_total, new_acc]
            return tuple(updated)

        return lax.cond(offset <= last_row, update, lambda inner: inner, running)

    final = lax.fori_loop(0, piece_rows // block_width, one_block, start_state)
    first_map = final[2] / final[1][:, :, None]
    second_map = final[5] / final[4][:, :, None]
    differ = first_map - lambdas[:, None, None] * second_map
    spread = lax.rsqrt(jnp.mean(differ * differ, axis=2, keepdims=True) + 1e-06)
    attended = (differ * spread * head_gain).astype(jnp.bfloat16)
    attended = jnp.transpose(attended, (1, 0, 2)).reshape(tok_rows, head_count * DV)
    all_heads = lax.all_to_all(attended, "tp", split_axis=0, concat_axis=1, tiled=True)
    projected = jnp.dot(all_heads, out_weight, preferred_element_type=jnp.float32).astype(
        jnp.bfloat16
    )
    resid = (tokens.astype(jnp.float32) + projected.astype(jnp.float32)).astype(jnp.bfloat16)
    resid_full = resid.astype(jnp.float32)
    normed = (
        resid_full
        * lax.rsqrt(jnp.mean(resid_full * resid_full, axis=1, keepdims=True) + 1e-06)
        * mixer_gain
    ).astype(jnp.bfloat16)
    up_full, down_full = (
        lax.all_gather(up_weight, "sp", axis=0, tiled=True),
        lax.all_gather(down_weight, "sp", axis=1, tiled=True),
    )
    hidden = jnp.square(
        jax.nn.relu(
            jnp.dot(
                lax.all_gather(normed, "tp", axis=0, tiled=True),
                up_full,
                preferred_element_type=jnp.float32,
            )
        )
    ).astype(jnp.bfloat16)
    mixed = lax.psum_scatter(
        jnp.dot(hidden, down_full, preferred_element_type=jnp.float32).astype(jnp.bfloat16),
        "tp",
        scatter_dimension=0,
        tiled=True,
    ).astype(jnp.float32)
    return (resid_full + mixed).astype(jnp.bfloat16)


def solution(mesh):
    placed = (
        P(("sp", "tp"), None),
        P("sp", "tp"),
        P("sp", "tp"),
        P("sp", "tp"),
        P("tp"),
        P(),
        P(),
        P(),
        P("sp", "tp"),
        P("tp", "sp"),
    )
    return jax.shard_map(
        per_device, mesh=mesh, in_specs=placed, out_specs=P(("sp", "tp"), None), check_vma=False
    )
```

profile of v0, /device:TPU:0, one launch (start us, length us, event | category | flops | bytes accessed | tf_op | source)
XLA Modules:
  0.0 390.4 jit_solution(7003081648482967234)
XLA Ops:
  6.5 0.0 all-gather.6.cloned.1.call-start
  6.5 1.8 copy.19
  8.3 0.0 all-gather.6.cloned.1.call-update
  8.4 0.0 all-gather.8.cloned.1.call-start
  8.4 1.8 copy.21
  10.2 0.0 all-gather.8.cloned.1.call-update
  10.2 0.0 all-gather.10.cloned.1.call-start
  10.3 1.1 copy.20
  11.4 51.1 %all-gather.6.cloned.1.call-done = bf16[4096,256]{0,1:T(8,128)(2,1)} async-done(((bf16[512,256]{0,1:T(8,128)(2,1)}), bf16[4096,256]{0,1:T(8,128)(2,1)}) %all-gather.6.cloned.1.call-update) | async-done | bytes 2097168 | tf_op jit(solution)/shard_map/all_gather | solution.py:35
  62.5 50.6 %all-gather.8.cloned.1.call-done = bf16[4096,256]{0,1:T(8,128)(2,1)} async-done(((bf16[512,256]{0,1:T(8,128)(2,1)}), bf16[4096,256]{0,1:T(8,128)(2,1)}) %all-gather.8.cloned.1.call-update) | async-done | bytes 2097168 | tf_op jit(solution)/shard_map/all_gather | solution.py:36
  113.2 0.0 copy-start.2
  113.2 0.0 copy-start.3
  113.2 6.1 %while.24 = (s32[]{:T(128)}, f32[2,512]{1,0:T(2,128)S(1)}, f32[2,512]{1,0:T(2,128)S(1)}, f32[2,512,128]{2,1,0:T(8,128)S(1)}, f32[2,512]{1,0:T(2,128)S(1)}, /*ind...) while((s32[]{:T(128)}, f32[2,512]{1,0:T(2,128)S(1)}, ...), condition=%wide.region_7.8_spmd.clone, body=%wide.region_0.7_spmd.clone.sunk | while | flops 410784768 | bytes 17707416 | solution.py:82
  113.3 5.6 %conditional.3 = ((f32[2,512]{1,0:T(2,128)S(1)}, f32[2,512]{1,0:T(2,128)S(1)}, f32[2,512,128]{2,1,0:T(8,128)S(1)}, f32[2,512]{1,0:T(2,128)S(1)}, f32[2,512]{1,0:T(2,128)S(1)}, /*index=5*/f32[2,512,128]{2,1,0:T(8,128)S(1)})) conditional(s32[]{:T(128)} %convert_element_type.94, (f32[2,512]{1,0:T(2,128)S(1)}, f32[2,512]{1,0:T(2,128)S(1)}, ...), branch_computations={%region_1.0_spmd, %region_2.6_spmd} | conditional | flops 410784768 | bytes 17705066 | solution.py:80
  113.3 1.0 constant_dynamic-slice_fusion.1
  114.3 0.2 broadcast_compare_fusion
  114.5 0.6 fusion.20
  115.2 0.3 fusion.3
  115.5 0.6 fusion.21
  116.1 0.3 fusion.5
  116.4 1.0 constant_dynamic-slice_fusion
  117.4 0.7 convolution_add_fusion
  118.1 0.7 convolution_add_fusion.1
  119.3 0.0 copy-done.2
  119.3 0.0 copy-start
  119.3 0.5 multiply_reduce_fusion.1
  119.9 0.0 copy-done.3
  119.9 0.2 fusion.18
  120.1 0.3 copy.23
  120.4 0.2 all_to_all.14
  120.5 8.5 %all_to_all.19 = bf16[4,128,256]{2,1,0:T(8,128)(2,1)S(1)} all-to-all(bf16[4,128,256]{2,1,0:T(8,128)(2,1)S(1)} %all_to_all.14), channel_id=1, replica_groups=mesh['sp'=8,'tp'=4] {'tp'}, dimensions={0} | all-to-all | bytes 524288 | tf_op jit(solution)/shard_map/all_to_all | solution.py:89
  129.1 0.2 copy.24
  129.3 0.0 copy-start.1
  129.3 3.0 multiply_reduce_fusion
  132.3 1.0 multiply_convert_fusion.1
  133.3 0.0 all-gather.10.cloned.1.call-update
  133.3 0.0 all-gather.12.cloned.1.call-start
  133.3 0.5 all-gather.12.cloned.1.call-update
  133.9 0.0 all-gather.14.cloned.1.call-start
  133.9 0.5 all-gather.14.cloned.1.call-update
  134.5 0.0 reduce-scatter.2.cloned.1.call-start
  134.5 57.8 %all-gather.10.cloned.1.call-done = bf16[512,2048]{1,0:T(8,128)(2,1)} async-done(((bf16[128,2048]{1,0:T(8,128)(2,1)}), bf16[512,2048]{1,0:T(8,128)(2,1)}) %all-gather.10.cloned.1.call-update) | async-done | bytes 2097168 | tf_op jit(solution)/shard_map/all_gather | solution.py:107
  192.3 74.8 %all-gather.12.cloned.1.call-done = bf16[2048,1024]{1,0:T(8,128)(2,1)} async-done(((bf16[256,1024]{1,0:T(8,128)(2,1)}), bf16[2048,1024]{1,0:T(8,128)(2,1)}) %all-gather.12.cloned.1.call-update) | async-done | bytes 4194320 | tf_op jit(solution)/shard_map/all_gather | solution.py:101
  267.1 75.1 %all-gather.14.cloned.1.call-done = bf16[1024,2048]{1,0:T(8,128)(2,1)} async-done(((bf16[1024,256]{1,0:T(8,128)(2,1)}), bf16[1024,2048]{1,0:T(8,128)(2,1)}) %all-gather.14.cloned.1.call-update) | async-done | bytes 4194320 | tf_op jit(solution)/shard_map/all_gather | solution.py:102
  342.2 9.9 %convolution_convert_fusion = bf16[512,2048]{1,0:T(8,128)(2,1)} fusion(bf16[1024,2048]{1,0:T(8,128)(2,1)} %all-gather.14.cloned.1.call-done, bf16[512,2048]{1,0:T(8,128)(2,1)} %all-gather.10.cloned.1.call-done, bf16[2048,1024]{1,0:T(8,128)(2,1)} %all-gather.12.cloned.1.call-done), kind=kOutput, calls=%fused_computation.28 | convolution fusion | flops 4297588736 | bytes 12582912 | tf_op jit(solution)/shard_map/dot_general | solution.py:114
  352.1 0.0 reduce-scatter.2.cloned.1.call-update
  352.1 29.5 %reduce-scatter.2.cloned.1.call-done = bf16[128,2048]{1,0:T(8,128)(2,1)} async-done(((bf16[512,2048]{1,0:T(8,128)(2,1)}), bf16[128,2048]{1,0:T(8,128)(2,1)}) %reduce-scatter.2.cloned.1.call-update) | async-done | bytes 524304 | tf_op jit(solution)/shard_map/reduce_scatter | solution.py:113
  381.6 1.9 add_convert_fusion
  (33 shorter events, 0.3 us)
Async XLA Ops:
  6.5 55.9 %all-gather.6.cloned.1.call-start = ((), (), s32[]{:S(2)}) async-start(), calls=%async_computation.2 | async-start | bytes 2359296 | tf_op jit(solution)/shard_map/all_gather | solution.py:35
  8.4 104.7 %all-gather.8.cloned.1.call-start = ((), (), s32[]{:S(2)}) async-start(), calls=%async_computation.3 | async-start | bytes 2359296 | tf_op jit(solution)/shard_map/all_gather | solution.py:36
  10.2 182.1 %all-gather.10.cloned.1.call-start = ((), (), s32[]{:S(2)}) async-start(), calls=%async_computation.4 | async-start | bytes 2621440 | tf_op jit(solution)/shard_map/all_gather | solution.py:107
  113.2 6.1 %copy-start.2 = (f32[2]{0:T(128)S(1)}, f32[2]{0:T(128)}, u32[]{:S(2)}) copy-start(f32[2]{0:T(128)} %param.18) | copy-start | bytes 28
  113.2 6.6 %copy-start.3 = (f32[128]{0:T(128)S(1)}, f32[128]{0:T(128)}, u32[]{:S(2)}) copy-start(f32[128]{0:T(128)} %param.19) | copy-start | bytes 1540
  119.3 9.9 %copy-start = (bf16[128,2048]{1,0:T(8,128)(2,1)S(1)}, bf16[128,2048]{1,0:T(8,128)(2,1)}, u32[]{:S(2)}) copy-start(bf16[128,2048]{1,0:T(8,128)(2,1)} %param.14) | copy-start | bytes 1572868
  129.3 3.0 copy-start.1
  133.3 133.8 %all-gather.12.cloned.1.call-start = ((), (), s32[]{:S(2)}) async-start(), calls=%async_computation.5 | async-start | bytes 4718592 | tf_op jit(solution)/shard_map/all_gather | solution.py:101
  133.9 208.3 %all-gather.14.cloned.1.call-start = ((), (), s32[]{:S(2)}) async-start(), calls=%async_computation.6 | async-start | bytes 4718592 | tf_op jit(solution)/shard_map/all_gather | solution.py:102
  134.5 247.2 %reduce-scatter.2.cloned.1.call-start = ((), (), s32[]{:S(2)}) async-start(), calls=%async_computation.7 | async-start | bytes 2621440 | tf_op jit(solution)/shard_map/reduce_scatter | solution.py:113
Sparse Core Ops, SparseCore 0:
  9.4 53.0 all-gather.5
  64.5 48.5 all-gather.7
  133.4 58.8 all-gather.9
  194.3 72.7 all-gather.11
  269.0 73.1 all-gather.13
  352.3 29.3 reduce-scatter.1
where the time goes:
time: 391 us; the launch traced here: 390 us
  waiting for transfers between devices  340 us (87%)
  matrix products  15.6 us (4%)
  between operations  13.6 us (3%)
  blocking collectives  8.55 us (2%)
  local copies, waits for them, and re-layouts  7.41 us (2%)
  other arithmetic  4.49 us (1%)
    all_gather x1, waiting for transfers between devices, per_device(): lax.all_gather(down_weight, 'sp', axis=1, tiled=True)  75.1 us
    all_gather x1, waiting for transfers between devices, per_device(): lax.all_gather(up_weight, 'sp', axis=0, tiled=True)  74.8 us
    all_gather x1, waiting for transfers between devices, per_device(): lax.all_gather(normed, 'tp', axis=0, tiled=True)  57.8 us
    all_gather x1, waiting for transfers between devices, per_device(): key_piece = lax.all_gather(keys, 'sp', axis=0, tiled=True)  51.1 us
    all_gather x1, waiting for transfers between devices, per_device(): value_piece = lax.all_gather(values, 'sp', axis=0, tiled=True)  50.6 us
    reduce_scatter x1, waiting for transfers between devices, per_device(): lax.psum_scatter(jnp.dot(hidden, down_full, preferred_element_type=jnp.fl...  29.5 us
    dot_general x1, matrix products, per_device(): jnp.dot(hidden, down_full, preferred_element_type=jnp.float32)  9.93 us
    all_to_all x1, blocking collectives, per_device(): lax.all_to_all(attended, 'tp', split_axis=0, concat_axis=1, tiled=True)  8.55 us
  transfers between devices with their start and end apart: 6, of which 6 were waited for; matrix products, arithmetic and copies ran while one was open for 1% of the time, Pallas kernels for 0%

commit v1 on v0

--- a/solution.py
+++ b/solution.py
@@ -32,7 +32,13 @@
     zero_total = jnp.zeros((head_count, tok_rows), jnp.float32)
     zero_acc = jnp.zeros((head_count, tok_rows, DV), jnp.float32)
     start_state = (floor_max, zero_total, zero_acc, floor_max, zero_total, zero_acc)
-    key_piece = lax.all_gather(keys, "sp", axis=0, tiled=True)
+    peers = lax.axis_size("sp")
+    block, blocks = (keys, [keys])
+    for _ in range(peers - 1):
+        block = lax.ppermute(block, "sp", [(i, (i + 1) % peers) for i in range(peers)])
+        blocks.insert(0, block)
+    flat = jnp.concatenate(blocks, axis=0)
+    key_piece = jnp.roll(flat, (lax.axis_index("sp") + 1) * keys.shape[0], axis=0)
     value_piece = lax.all_gather(values, "sp", axis=0, tiled=True)
     piece_rows = key_piece.shape[0]
     block_width = math.gcd(piece_rows, 512)

time: 391 us -> 365 us (0.934)
  waiting for transfers between devices: 340 us -> 311 us
    ppermute x0 -> x7, waiting for transfers between devices: none -> 78.5 us  [per_device(): lax.ppermute(block, 'sp', [(i, (i + 1) % peers) for i in range(peers)])]
    all_gather x1 -> x0, waiting for transfers between devices: 51.1 us -> none  [per_device(): key_piece = lax.all_gather(keys, 'sp', axis=0, tiled=True)]
    all_gather x1, waiting for transfers between devices: 50.6 us -> 1.34 us  [per_device(): value_piece = lax.all_gather(values, 'sp', axis=0, tiled=True)]
    all_gather x1, waiting for transfers between devices: 57.8 us -> 50.6 us  [per_device(): lax.all_gather(normed, 'tp', axis=0, tiled=True)]
  transfers between devices with their start and end apart: 6 -> 12, of which waited for: 6 -> 12; matrix products, arithmetic and copies ran while one was open for 1% -> 1% of each run, Pallas kernels for 0% -> 0%
where the time goes in v1:
time: 365 us; the launch traced here: 364 us
  waiting for transfers between devices  311 us (85%)
  matrix products  15.6 us (4%)
  between operations  13.5 us (4%)
  blocking collectives  9.58 us (3%)
  local copies, waits for them, and re-layouts  6.36 us (2%)
  other arithmetic  4.49 us (1%)
    ppermute x7, waiting for transfers between devices, per_device(): lax.ppermute(block, 'sp', [(i, (i + 1) % peers) for i in range(peers)])  78.5 us
    all_gather x1, waiting for transfers between devices, per_device(): lax.all_gather(down_weight, 'sp', axis=1, tiled=True)  76.7 us
    all_gather x1, waiting for transfers between devices, per_device(): lax.all_gather(up_weight, 'sp', axis=0, tiled=True)  73 us
    all_gather x1, waiting for transfers between devices, per_device(): lax.all_gather(normed, 'tp', axis=0, tiled=True)  50.6 us
    reduce_scatter x1, waiting for transfers between devices, per_device(): lax.psum_scatter(jnp.dot(hidden, down_full, preferred_element_type=jnp.fl...  29.8 us
    dot_general x1, matrix products, per_device(): jnp.dot(hidden, down_full, preferred_element_type=jnp.float32)  9.94 us
    all_to_all x1, blocking collectives, per_device(): lax.all_to_all(attended, 'tp', split_axis=0, concat_axis=1, tiled=True)  9.58 us
  transfers between devices with their start and end apart: 12, of which 12 were waited for; matrix products, arithmetic and copies ran while one was open for 1% of the time, Pallas kernels for 0%

profile of v1, /device:TPU:0, one launch (start us, length us, event | category | flops | bytes accessed | tf_op | source)
XLA Modules:
  0.0 364.5 jit_solution(16382751065413296117)
XLA Ops:
  6.5 1.1 copy.19
  7.6 3.0 collective-permute-start
  10.7 9.3 %collective-permute-done = bf16[512,256]{0,1:T(8,128)(2,1)S(1)} collective-permute-done((bf16[512,256]{0,1:T(8,128)(2,1)S(1)}, bf16[512,256]{0,1:T(8,128)(2,1)S(1)}, u32[]{:S(2)}, u32[]{:S(2)}) %collective-permute-start) | collective-permute-done | bytes 262176 | tf_op jit(solution)/shard_map/ppermute | solution.py:38
  20.0 10.2 %collective-permute-done.1 = bf16[512,256]{0,1:T(8,128)(2,1)S(1)} collective-permute-done((bf16[512,256]{0,1:T(8,128)(2,1)S(1)}, bf16[512,256]{0,1:T(8,128)(2,1)S(1)}, u32[]{:S(2)}, u32[]{:S(2)}) %collective-permute-start.1) | collective-permute-done | bytes 262176 | tf_op jit(solution)/shard_map/ppermute | solution.py:38
  30.2 1.8 copy.23
  32.0 0.0 all-gather.5.cloned.1.call-update
  32.0 0.0 all-gather.7.cloned.1.call-start
  32.1 7.4 %collective-permute-done.2 = bf16[512,256]{0,1:T(8,128)(2,1)S(1)} collective-permute-done((bf16[512,256]{0,1:T(8,128)(2,1)S(1)}, bf16[512,256]{0,1:T(8,128)(2,1)S(1)}, u32[]{:S(2)}, u32[]{:S(2)}) %collective-permute-start.2) | collective-permute-done | bytes 262176 | tf_op jit(solution)/shard_map/ppermute | solution.py:38
  39.5 12.4 %collective-permute-done.3 = bf16[512,256]{0,1:T(8,128)(2,1)S(1)} collective-permute-done((bf16[512,256]{0,1:T(8,128)(2,1)S(1)}, bf16[512,256]{0,1:T(8,128)(2,1)S(1)}, u32[]{:S(2)}, u32[]{:S(2)}) %collective-permute-start.3) | collective-permute-done | bytes 262176 | tf_op jit(solution)/shard_map/ppermute | solution.py:38
  51.9 12.0 %collective-permute-done.4 = bf16[512,256]{0,1:T(8,128)(2,1)S(1)} collective-permute-done((bf16[512,256]{0,1:T(8,128)(2,1)S(1)}, bf16[512,256]{0,1:T(8,128)(2,1)S(1)}, u32[]{:S(2)}, u32[]{:S(2)}) %collective-permute-start.4) | collective-permute-done | bytes 262176 | tf_op jit(solution)/shard_map/ppermute | solution.py:38
  63.9 13.5 %collective-permute-done.5 = bf16[512,256]{0,1:T(8,128)(2,1)S(1)} collective-permute-done((bf16[512,256]{0,1:T(8,128)(2,1)S(1)}, bf16[512,256]{0,1:T(8,128)(2,1)S(1)}, u32[]{:S(2)}, u32[]{:S(2)}) %collective-permute-start.5) | collective-permute-done | bytes 262176 | tf_op jit(solution)/shard_map/ppermute | solution.py:38
  77.4 1.1 copy.22
  78.5 13.7 %collective-permute-done.6 = bf16[512,256]{0,1:T(8,128)(2,1)S(1)} collective-permute-done((bf16[512,256]{0,1:T(8,128)(2,1)S(1)}, bf16[512,256]{0,1:T(8,128)(2,1)S(1)}, u32[]{:S(2)}, u32[]{:S(2)}) %collective-permute-start.6) | collective-permute-done | bytes 262176 | tf_op jit(solution)/shard_map/ppermute | solution.py:38
  92.8 0.1 constant_dynamic-slice_fusion.2
  92.9 1.3 all-gather.5.cloned.1.call-done
  94.4 0.0 copy-start.2
  94.4 5.1 %while.24 = (s32[]{:T(128)}, f32[2,512]{1,0:T(2,128)S(1)}, f32[2,512]{1,0:T(2,128)S(1)}, f32[2,512,128]{2,1,0:T(8,128)S(1)}, f32[2,512]{1,0:T(2,128)S(1)}, /*ind...) while((s32[]{:T(128)}, f32[2,512]{1,0:T(2,128)S(1)}, ...), condition=%wide.region_7.8_spmd.clone, body=%wide.region_0.7_spmd.clone.sunk | while | flops 410784768 | bytes 17707416 | solution.py:88
  94.5 4.7 %conditional.3 = ((f32[2,512]{1,0:T(2,128)S(1)}, f32[2,512]{1,0:T(2,128)S(1)}, f32[2,512,128]{2,1,0:T(8,128)S(1)}, f32[2,512]{1,0:T(2,128)S(1)}, f32[2,512]{1,0:T(2,128)S(1)}, /*index=5*/f32[2,512,128]{2,1,0:T(8,128)S(1)})) conditional(s32[]{:T(128)} %convert_element_type.94, (f32[2,512]{1,0:T(2,128)S(1)}, f32[2,512]{1,0:T(2,128)S(1)}, ...), branch_computations={%region_1.1_spmd, %region_2.6_spmd} | conditional | flops 410784768 | bytes 17705066 | solution.py:86
  94.5 0.2 broadcast_compare_fusion
  94.8 0.6 fusion.20
  95.4 0.3 fusion.3
  95.7 0.6 fusion.21
  96.3 0.3 fusion.5
  96.7 1.0 constant_dynamic-slice_fusion
  97.7 0.7 convolution_add_fusion
  98.4 0.7 convolution_add_fusion.1
  99.5 0.0 copy-start
  99.6 0.5 multiply_reduce_fusion.1
  100.1 0.2 fusion.18
  100.3 0.3 copy.25
  100.6 0.2 all_to_all.14
  100.8 9.6 %all_to_all.19 = bf16[4,128,256]{2,1,0:T(8,128)(2,1)S(1)} all-to-all(bf16[4,128,256]{2,1,0:T(8,128)(2,1)S(1)} %all_to_all.14), channel_id=1, replica_groups=mesh['sp'=8,'tp'=4] {'tp'}, dimensions={0} | all-to-all | bytes 524288 | tf_op jit(solution)/shard_map/all_to_all | solution.py:95
  110.4 0.2 copy.26
  110.6 3.0 multiply_reduce_fusion
  113.6 1.0 multiply_convert_fusion.1
  114.6 0.0 all-gather.7.cloned.1.call-update
  114.6 0.0 all-gather.11.cloned.1.call-start
  114.6 0.7 all-gather.11.cloned.1.call-update
  115.3 0.0 all-gather.9.cloned.1.call-start
  115.4 0.5 all-gather.9.cloned.1.call-update
  115.9 0.0 reduce-scatter.2.cloned.1.call-start
  115.9 50.6 %all-gather.7.cloned.1.call-done = bf16[512,2048]{1,0:T(8,128)(2,1)} async-done(((bf16[128,2048]{1,0:T(8,128)(2,1)}), bf16[512,2048]{1,0:T(8,128)(2,1)}) %all-gather.7.cloned.1.call-update) | async-done | bytes 2097168 | tf_op jit(solution)/shard_map/all_gather | solution.py:113
  166.5 76.7 %all-gather.11.cloned.1.call-done = bf16[1024,2048]{1,0:T(8,128)(2,1)} async-done(((bf16[1024,256]{1,0:T(8,128)(2,1)}), bf16[1024,2048]{1,0:T(8,128)(2,1)}) %all-gather.11.cloned.1.call-update) | async-done | bytes 4194320 | tf_op jit(solution)/shard_map/all_gather | solution.py:108
  243.2 73.0 %all-gather.9.cloned.1.call-done = bf16[2048,1024]{1,0:T(8,128)(2,1)} async-done(((bf16[256,1024]{1,0:T(8,128)(2,1)}), bf16[2048,1024]{1,0:T(8,128)(2,1)}) %all-gather.9.cloned.1.call-update) | async-done | bytes 4194320 | tf_op jit(solution)/shard_map/all_gather | solution.py:107
  316.2 9.9 %convolution_convert_fusion = bf16[512,2048]{1,0:T(8,128)(2,1)} fusion(bf16[1024,2048]{1,0:T(8,128)(2,1)} %all-gather.11.cloned.1.call-done, bf16[512,2048]{1,0:T(8,128)(2,1)} %all-gather.7.cloned.1.call-done, bf16[2048,1024]{1,0:T(8,128)(2,1)} %all-gather.9.cloned.1.call-done), kind=kOutput, calls=%fused_computation.28 | convolution fusion | flops 4297588736 | bytes 12582912 | tf_op jit(solution)/shard_map/dot_general | solution.py:120
  326.1 0.0 reduce-scatter.2.cloned.1.call-update
  326.2 29.8 %reduce-scatter.2.cloned.1.call-done = bf16[128,2048]{1,0:T(8,128)(2,1)} async-done(((bf16[512,2048]{1,0:T(8,128)(2,1)}), bf16[128,2048]{1,0:T(8,128)(2,1)}) %reduce-scatter.2.cloned.1.call-update) | async-done | bytes 524304 | tf_op jit(solution)/shard_map/reduce_scatter | solution.py:119
  356.0 1.9 add_convert_fusion
  (61 shorter events, 0.8 us)
Async XLA Ops:
  6.5 87.7 %all-gather.5.cloned.1.call-start = ((), (), s32[]{:S(2)}) async-start(), calls=%async_computation.2 | async-start | bytes 2359296 | tf_op jit(solution)/shard_map/all_gather | solution.py:42
  7.6 12.4 %collective-permute-start = (bf16[512,256]{0,1:T(8,128)(2,1)S(1)}, bf16[512,256]{0,1:T(8,128)(2,1)S(1)}, u32[]{:S(2)}, u32[]{:S(2)}) collective-permute-start(bf16[512,256]{0,1:T(8,128)(2,1)S(1)} %copy.19), channel_id=1, source_target_pairs={{0,4},{4,8},{8,12},{12,16},{16,20},{20,24},{24,28},{28,0},{1,5},{5... | collective-permute-start | bytes 786440 | tf_op jit(solution)/shard_map/ppermute | solution.py:38
  20.0 10.2 %collective-permute-start.1 = (bf16[512,256]{0,1:T(8,128)(2,1)S(1)}, bf16[512,256]{0,1:T(8,128)(2,1)S(1)}, u32[]{:S(2)}, u32[]{:S(2)}) collective-permute-start(bf16[512,256]{0,1:T(8,128)(2,1)S(1)} %collective-permute-done), channel_id=1, source_target_pairs={{0,4},{4,8},{8,12},{12,16},{16,20},{20,24},{24,28},{28,0},{1,5},{5... | collective-permute-start | bytes 786440 | tf_op jit(solution)/shard_map/ppermute | solution.py:38
  30.2 9.3 %collective-permute-start.2 = (bf16[512,256]{0,1:T(8,128)(2,1)S(1)}, bf16[512,256]{0,1:T(8,128)(2,1)S(1)}, u32[]{:S(2)}, u32[]{:S(2)}) collective-permute-start(bf16[512,256]{0,1:T(8,128)(2,1)S(1)} %collective-permute-done.1), channel_id=1, source_target_pairs={{0,4},{4,8},{8,12},{12,16},{16,20},{20,24},{24,28},{28,0},{1,5},{5... | collective-permute-start | bytes 786440 | tf_op jit(solution)/shard_map/ppermute | solution.py:38
  32.0 134.5 %all-gather.7.cloned.1.call-start = ((), (), s32[]{:S(2)}) async-start(), calls=%async_computation.3 | async-start | bytes 2621440 | tf_op jit(solution)/shard_map/all_gather | solution.py:113
  39.5 12.4 %collective-permute-start.3 = (bf16[512,256]{0,1:T(8,128)(2,1)S(1)}, bf16[512,256]{0,1:T(8,128)(2,1)S(1)}, u32[]{:S(2)}, u32[]{:S(2)}) collective-permute-start(bf16[512,256]{0,1:T(8,128)(2,1)S(1)} %collective-permute-done.2), channel_id=1, source_target_pairs={{0,4},{4,8},{8,12},{12,16},{16,20},{20,24},{24,28},{28,0},{1,5},{5... | collective-permute-start | bytes 786440 | tf_op jit(solution)/shard_map/ppermute | solution.py:38
  51.9 12.0 %collective-permute-start.4 = (bf16[512,256]{0,1:T(8,128)(2,1)S(1)}, bf16[512,256]{0,1:T(8,128)(2,1)S(1)}, u32[]{:S(2)}, u32[]{:S(2)}) collective-permute-start(bf16[512,256]{0,1:T(8,128)(2,1)S(1)} %collective-permute-done.3), channel_id=1, source_target_pairs={{0,4},{4,8},{8,12},{12,16},{16,20},{20,24},{24,28},{28,0},{1,5},{5... | collective-permute-start | bytes 786440 | tf_op jit(solution)/shard_map/ppermute | solution.py:38
  63.9 13.5 %collective-permute-start.5 = (bf16[512,256]{0,1:T(8,128)(2,1)S(1)}, bf16[512,256]{0,1:T(8,128)(2,1)S(1)}, u32[]{:S(2)}, u32[]{:S(2)}) collective-permute-start(bf16[512,256]{0,1:T(8,128)(2,1)S(1)} %collective-permute-done.4), channel_id=1, source_target_pairs={{0,4},{4,8},{8,12},{12,16},{16,20},{20,24},{24,28},{28,0},{1,5},{5... | collective-permute-start | bytes 786440 | tf_op jit(solution)/shard_map/ppermute | solution.py:38
  77.4 14.8 %collective-permute-start.6 = (bf16[512,256]{0,1:T(8,128)(2,1)S(1)}, bf16[512,256]{0,1:T(8,128)(2,1)S(1)}, u32[]{:S(2)}, u32[]{:S(2)}) collective-permute-start(bf16[512,256]{0,1:T(8,128)(2,1)S(1)} %collective-permute-done.5), channel_id=1, source_target_pairs={{0,4},{4,8},{8,12},{12,16},{16,20},{20,24},{24,28},{28,0},{1,5},{5... | collective-permute-start | bytes 786440 | tf_op jit(solution)/shard_map/ppermute | solution.py:38
  94.4 5.2 %copy-start.2 = (f32[2]{0:T(128)S(1)}, f32[2]{0:T(128)}, u32[]{:S(2)}) copy-start(f32[2]{0:T(128)} %param.18) | copy-start | bytes 28
  94.4 5.7 %copy-start.3 = (f32[128]{0:T(128)S(1)}, f32[128]{0:T(128)}, u32[]{:S(2)}) copy-start(f32[128]{0:T(128)} %param.19) | copy-start | bytes 1540
  99.5 11.0 %copy-start = (bf16[128,2048]{1,0:T(8,128)(2,1)S(1)}, bf16[128,2048]{1,0:T(8,128)(2,1)}, u32[]{:S(2)}) copy-start(bf16[128,2048]{1,0:T(8,128)(2,1)} %param.14) | copy-start | bytes 1572868
  100.3 13.3 %copy-start.1 = (f32[2048]{0:T(1024)S(1)}, f32[2048]{0:T(1024)}, u32[]{:S(2)}) copy-start(f32[2048]{0:T(1024)} %param.21) | copy-start | bytes 24580
  114.6 128.6 %all-gather.11.cloned.1.call-start = ((), (), s32[]{:S(2)}) async-start(), calls=%async_computation.5 | async-start | bytes 4718592 | tf_op jit(solution)/shard_map/all_gather | solution.py:108
  115.3 200.9 %all-gather.9.cloned.1.call-start = ((), (), s32[]{:S(2)}) async-start(), calls=%async_computation.4 | async-start | bytes 4718592 | tf_op jit(solution)/shard_map/all_gather | solution.py:107
  115.9 240.1 %reduce-scatter.2.cloned.1.call-start = ((), (), s32[]{:S(2)}) async-start(), calls=%async_computation.6 | async-start | bytes 2621440 | tf_op jit(solution)/shard_map/reduce_scatter | solution.py:119
Sparse Core Ops, SparseCore 0:
  32.1 62.0 all-gather.4
  114.7 51.7 all-gather.6
  168.5 74.6 all-gather.10
  245.2 70.9 all-gather.8
  326.3 29.6 reduce-scatter.1
